TPU v7x, 32 devices: a whole 2x2x4 slice. The times are simulated.
32 devices in a mesh: sp: 8 (over z, x), tp: 4 (over y, core).
Axes of the slice: x: 2, y: 2, z: 4, core: 2. Of those that a mesh axis runs over, the one named last changes fastest.
Arguments:
- target: bfloat16 [4096, 4096], P(('sp', 'tp')), may hold values from -0.07 to 0.07
- source: bfloat16 [8192, 4096], P(('sp', 'tp')), may hold values from -0.035 to 0.035
- gain_target: float32 [4096], replicated, may hold values from 0.1 to 1.9
- gain_source: float32 [4096], replicated, may hold values from 0.1 to 1.9
- w_query: bfloat16 [4096, 1024], P(None, 'tp'), may hold values from -1 to 1
- w_key: bfloat16 [4096, 512], replicated, may hold values from -1 to 1
- w_value: bfloat16 [4096, 512], replicated, may hold values from -0.09375 to 0.09375
- w_out: bfloat16 [1024, 4096], P('tp'), may hold values from -0.1875 to 0.1875
- grad_output: bfloat16 [4096, 4096], P(('sp', 'tp')), may hold values from -6 to 6
Outputs:
- grad_target: float32 [4096, 4096], P(('sp', 'tp'))
- grad_source: float32 [8192, 4096], P(('sp', 'tp'))
- grad_out_proj: float32 [1024, 4096], P('tp')
All inputs are finite; a program needn't handle non-finite values.
Results may differ from a plain program's by a relative error of at most 0.028.
Values may be sent and summed in bfloat16 or wider, within the bound.
A program may use at most 128 MiB of HBM per device.

v0:
```python
import math

import jax
import jax.numpy as jnp
from jax import lax
from jax.sharding import PartitionSpec as P

HD = 64


EPS = 1e-06


def normalize(matrix, scaling):
    widened = matrix.astype(jnp.float32)
    factor = lax.rsqrt(jnp.mean(widened * widened, axis=-1, keepdims=True) + EPS)
    return (widened * factor * scaling).astype(jnp.bfloat16)


def norm_back(matrix, scaling, upstream):
    widened = matrix.astype(jnp.float32)
    factor = lax.rsqrt(jnp.mean(widened * widened, axis=-1, keepdims=True) + EPS)
    weighted = upstream * scaling
    inner = jnp.mean(widened * weighted, axis=-1, keepdims=True)
    return factor * weighted - widened * factor * factor * factor * inner


def score_block(queries, key_block, score_scale):
    return (
        jnp.einsum(
            "tkgd,skd->kgts", queries, key_block[:, :, 0], preferred_element_type=jnp.float32
        )
        * score_scale
    )


def split_arrived(arrived, key_count):
    row_count = arrived.shape[0]
    block_size = math.gcd(row_count, 1024)
    return (arrived.reshape(row_count // block_size, block_size, key_count, 2, HD), block_size)


def shards(target, source, gain_target, gain_source, w_query, w_key, w_value, w_out, grad_output):
    contract_last = (((1,), (1,)), ((), ()))
    across = lax.axis_size("tp")
    heads_all = w_key.shape[1] // HD
    key_count = heads_all // across
    query_count = w_query.shape[1] // HD
    group_size = query_count // key_count
    score_scale = float(HD) ** (-0.5)
    normed_target = normalize(target, gain_target)
    normed_source = normalize(source, gain_source)
    gathered_target, gathered_grad = (
        lax.all_gather(normed_target, "tp", axis=0, tiled=True),
        lax.all_gather(grad_output, "tp", axis=0, tiled=True),
    )
    query = jnp.dot(gathered_target, w_query, preferred_element_type=jnp.float32).astype(
        jnp.bfloat16
    )
    head_grads = lax.dot_general(
        gathered_grad, w_out, contract_last, preferred_element_type=jnp.float32
    ).astype(jnp.bfloat16)
    row_count = query.shape[0]
    queries = query.reshape(row_count, key_count, group_size, HD)
    grad_heads = head_grads.reshape(row_count, key_count, group_size, HD)
    w_both = jnp.stack(
        [w_key.reshape(-1, heads_all, HD), w_value.reshape(-1, heads_all, HD)], axis=2
    )
    w_both = w_both.reshape(w_key.shape[0], heads_all * 2 * HD)
    pairs = jnp.dot(normed_source, w_both, preferred_element_type=jnp.float32).astype(jnp.bfloat16)
    own_pairs = lax.all_to_all(pairs, "tp", split_axis=1, concat_axis=0, tiled=True)
    start_max = jnp.full((key_count, group_size, row_count), -jnp.inf, jnp.float32)
    start_sum = jnp.zeros((key_count, group_size, row_count), jnp.float32)
    start_acc = jnp.zeros((row_count, key_count, group_size, HD), jnp.float32)
    blocks, block_size = split_arrived(
        lax.all_gather(own_pairs, "sp", axis=0, tiled=True), key_count
    )

    def absorb_advance(status, key_block):
        maxima, totals, accum = status
        scores = score_block(queries, key_block, score_scale)
        new_max = jnp.maximum(maxima, jnp.max(scores, axis=-1))
        shrink = jnp.exp(maxima - new_max)
        weights = jnp.exp(scores - new_max[..., None])
        totals = totals * shrink + jnp.sum(weights, axis=-1)
        partial_value = jnp.einsum(
            "kgts,skd->tkgd",
            weights.astype(jnp.bfloat16),
            key_block[:, :, 1],
            preferred_element_type=jnp.float32,
        )
        accum = accum * jnp.transpose(shrink, (2, 0, 1))[..., None] + partial_value
        return ((new_max, totals, accum), None)

    result, _ = lax.scan(absorb_advance, (start_max, start_sum, start_acc), blocks)
    maxima, totals, accum = result
    attn_heads = (accum / jnp.transpose(totals, (2, 0, 1))[..., None]).astype(jnp.bfloat16)
    delta_sum = jnp.sum(grad_heads.astype(jnp.float32) * attn_heads.astype(jnp.float32), axis=-1)
    delta_sum = jnp.transpose(delta_sum, (1, 2, 0))
    all_rows = own_pairs.shape[0] * lax.axis_size("sp")
    start_grad = jnp.zeros((row_count, key_count, group_size, HD), jnp.float32)
    start_pairs = jnp.zeros((all_rows, key_count * 2 * HD), jnp.float32)
    blocks, block_size = split_arrived(
        lax.all_gather(own_pairs, "sp", axis=0, tiled=True), key_count
    )

    def collect_advance(status, bundle):
        query_grad, pair_store = status
        key_block, position = bundle
        scores = score_block(queries, key_block, score_scale)
        attend = jnp.exp(scores - maxima[..., None]) / totals[..., None]
        grad_attend = jnp.einsum(
            "tkgd,skd->kgts", grad_heads, key_block[:, :, 1], preferred_element_type=jnp.float32
        )
        mixed = (attend * (grad_attend - delta_sum[..., None]) * score_scale).astype(jnp.bfloat16)
        query_grad = query_grad + jnp.einsum(
            "kgts,skd->tkgd", mixed, key_block[:, :, 0], preferred_element_type=jnp.float32
        )
        grad_key = jnp.einsum("kgts,tkgd->skd", mixed, queries, preferred_element_type=jnp.float32)
        grad_value = jnp.einsum(
            "kgts,tkgd->skd",
            attend.astype(jnp.bfloat16),
            grad_heads,
            preferred_element_type=jnp.float32,
        )
        stacked = jnp.stack([grad_key, grad_value], axis=2).reshape(block_size, key_count * 2 * HD)
        where_rows = position * block_size
        pair_store = lax.dynamic_update_slice_in_dim(pair_store, stacked, where_rows, 0)
        return ((query_grad, pair_store), None)

    positions = jnp.arange(blocks.shape[0], dtype=jnp.int32)
    result, _ = lax.scan(collect_advance, (start_grad, start_pairs), (blocks, positions))
    query_grad, pair_store = result
    pair_grads = lax.psum_scatter(
        pair_store.astype(jnp.bfloat16), "sp", scatter_dimension=0, tiled=True
    )
    grad_query = query_grad.astype(jnp.bfloat16).reshape(row_count, query_count * HD)
    pair_rows = lax.all_to_all(pair_grads, "tp", split_axis=0, concat_axis=1, tiled=True)
    grad_sn = lax.dot_general(pair_rows, w_both, contract_last, preferred_element_type=jnp.float32)
    grad_source = norm_back(source, gain_source, grad_sn)
    attention = attn_heads.reshape(row_count, query_count * HD)
    proj_part = lax.dot_general(
        attention, gathered_grad, (((0,), (0,)), ((), ())), preferred_element_type=jnp.float32
    )
    grad_out_proj = lax.psum(proj_part.astype(jnp.bfloat16), "sp").astype(jnp.float32)
    grad_xn = lax.psum_scatter(
        lax.dot_general(
            grad_query, w_query, contract_last, preferred_element_type=jnp.float32
        ).astype(jnp.bfloat16),
        "tp",
        scatter_dimension=0,
        tiled=True,
    ).astype(jnp.float32)
    grad_target = norm_back(target, gain_target, grad_xn)
    return (grad_target, grad_source, grad_out_proj)


def solution(mesh):
    return jax.shard_map(
        shards,
        mesh=mesh,
        in_specs=(
            P(("sp", "tp"), None),
            P(("sp", "tp"), None),
            P(),
            P(),
            P(None, "tp"),
            P(),
            P(),
            P("tp", None),
            P(("sp", "tp"), None),
        ),
        out_specs=(P(("sp", "tp"), None), P(("sp", "tp"), None), P("tp", None)),
        check_vma=False,
    )
```

profile of v0, /device:TPU:0, one launch (start us, length us, event | category | flops | bytes accessed | tf_op | source)
XLA Modules:
  0.0 497.9 jit_solution(10498853188930583228)
XLA Ops:
  12.0 6.3 %copy.33 = bf16[4096,512]{0,1:T(8,128)(2,1)} copy(bf16[4096,512]{1,0:T(8,128)(2,1)} %param.18) | data formatting | bytes 8388608 | tf_op args[5]
  18.3 6.4 %copy.34 = bf16[4096,512]{0,1:T(8,128)(2,1)} copy(bf16[4096,512]{1,0:T(8,128)(2,1)} %param.19) | data formatting | bytes 8388608 | tf_op args[6]
  24.7 7.5 %pad_maximum_fusion.1 = bf16[4096,8,2,64]{0,3,1,2:T(8,128)(2,1)} fusion(bf16[4096,8,1,64]{0,3,1,2:T(8,128)(2,1)} %bitcast.180, bf16[4096,8,1,64]{0,3,1,2:T(8,128)(2,1)} %bitcast.179), kind=kLoop, calls=%fused_computation.38 | loop fusion | flops 4194304 | bytes 16777216 | tf_op jit(solution)/shard_map/stack | solution.py:66
  32.2 7.9 %copy.35 = bf16[4096,8,2,64]{0,3,2,1:T(8,128)(2,1)} copy(bf16[4096,8,2,64]{0,3,1,2:T(8,128)(2,1)} %pad_maximum_fusion.1) | data formatting | bytes 16777216 | tf_op jit(solution)/shard_map/stack | solution.py:66
  40.7 5.8 %fusion.47 = bf16[256,1024]{1,0:T(8,128)(2,1)S(1)} fusion(bf16[4096,1024]{0,1:T(8,128)(2,1)} %bitcast.176, bf16[256,4096]{1,0:T(8,128)(2,1)S(1)} %copy-done.1, f32[4096]{0:T(1024)S(1)} %copy-done.6, f32[256]{0:T(256)S(1)} %add_rsqrt_fusion), kind=kOutput, calls=%fused_computation.68 | convolution fusion | flops 2151940096 | bytes 11027456 | tf_op jit(solution)/shard_map/dot_general | solution.py:70
  46.5 13.2 %all_to_all.38 = bf16[256,4,256]{2,0,1:T(8,128)(2,1)} all-to-all(bf16[256,4,256]{2,0,1:T(8,128)(2,1)S(1)} %bitcast.183), channel_id=1, replica_groups=mesh['sp'=8,'tp'=4] {'tp'}, dimensions={1} | all-to-all | bytes 1048576 | tf_op jit(solution)/shard_map/all_to_all | solution.py:71
  60.8 4.2 convolution_convert_fusion.3
  65.0 68.3 %all-gather.4.cloned.1.call-done = bf16[8192,256]{1,0:T(8,128)(2,1)} async-done(((bf16[1024,256]{1,0:T(8,128)(2,1)}), bf16[8192,256]{1,0:T(8,128)(2,1)}) %all-gather.4.cloned.1.call-update) | async-done | bytes 4194320 | tf_op jit(solution)/shard_map/all_gather | solution.py:104
  133.3 15.1 %reshape.81 = bf16[8,1024,2,2,64]{4,3,2,1,0:T(2,128)(2,1)} reshape(bf16[8192,256]{1,0:T(8,128)(2,1)} %all-gather.4.cloned.1.call-done) | data formatting | bytes 8388608 | tf_op jit(solution)/shard_map/reshape | solution.py:40
  148.4 20.1 %copy.39 = bf16[8,1024,2,2,64]{1,4,2,3,0:T(8,128)(2,1)} copy(bf16[8,1024,2,2,64]{4,3,2,1,0:T(2,128)(2,1)} %reshape.81) | data formatting | bytes 8388608
  168.5 51.7 %while.28 = (s32[]{:T(128)}, f32[2,2,512]{2,1,0:T(2,128)S(1)}, f32[2,2,512]{2,1,0:T(2,128)S(1)}, f32[512,2,2,64]{0,3,2,1:T(8,128)S(1)}, bf16[8,1024,2,2,64]{1,4,...) while((s32[]{:T(128)}, f32[2,2,512]{2,1,0:T(2,128)S(1)}, ...), condition=%wide.region_5.6_spmd.clone, body=%wide.region_2.5_spmd.clone.sunk | while | flops 554053632 | bytes 28180588 | solution.py:95
  220.3 4.3 multiply_reduce_fusion
  229.8 111.1 %while.29 = (s32[]{:T(128)}, f32[512,2,2,64]{0,3,2,1:T(8,128)}, bf16[8192,256]{1,0:T(8,128)(2,1)}, bf16[8,1024,2,2,64]{1,4,2,3,0:T(8,128)(2,1)}, bf16[512,2,2,64...) while((s32[]{:T(128)}, f32[512,2,2,64]{0,3,2,1:T(8,128)}, ...), condition=%wide.region_8.9_spmd.clone, body=%wide.region_7.8_spmd.clone.sunk | while | flops 1359478784 | bytes 46424276 | solution.py:132
  245.1 2.7 fusion.99
  250.6 2.7 fusion.101
  259.2 2.7 fusion.99
  264.6 2.7 fusion.101
  278.6 2.7 fusion.101
  292.7 2.7 fusion.101
  301.2 2.7 fusion.99
  306.7 2.7 fusion.101
  320.7 2.7 fusion.101
  329.3 2.7 fusion.99
  334.7 2.7 fusion.101
  342.1 3.3 convolution_convert_fusion
  345.4 4.5 convert_element_type.74
  349.9 77.9 %reduce-scatter.5.cloned.1.call-done = bf16[1024,256]{1,0:T(8,128)(2,1)} async-done(((bf16[8192,256]{1,0:T(8,128)(2,1)}), bf16[1024,256]{1,0:T(8,128)(2,1)}) %reduce-scatter.5.cloned.1.call-update) | async-done | bytes 524304 | tf_op jit(solution)/shard_map/reduce_scatter | solution.py:134
  427.9 4.5 all-to-all-start.1
  432.4 42.1 %reduce-scatter.3.cloned.1.call-done = bf16[128,4096]{1,0:T(8,128)(2,1)} async-done(((bf16[512,4096]{1,0:T(8,128)(2,1)}), bf16[128,4096]{1,0:T(8,128)(2,1)}) %reduce-scatter.3.cloned.1.call-update) | async-done | bytes 1048592 | tf_op jit(solution)/shard_map/reduce_scatter | solution.py:146
  476.2 3.2 fusion.40
  480.7 7.2 %fusion.34 = (f32[256]{0:T(256)S(1)}, f32[256,4096]{1,0:T(8,128)S(1)}) fusion(bf16[256,4096]{1,0:T(8,128)(2,1)} %param.14, f32[4096]{0:T(1024)S(1)} %copy-done.7, bf16[256,1024]{0,1:T(8,128)(2,1)S(1)} %bitcast.181, bf16[4096,1024]{0,1:T(8,128)(2,1)} %bitcast.177), kind=kOutput, calls=%fused_computation.52 | convolution fusion | flops 2151677696 | bytes 15221760 | tf_op jit(solution)/shard_map/dot_general | solution.py:139
  487.8 3.2 fusion.32
  (191 shorter events, 142.6 us)
Async XLA Ops:
  7.2 53.6 %copy-start = (bf16[4096,256]{1,0:T(8,128)(2,1)S(1)}, bf16[4096,256]{1,0:T(8,128)(2,1)}, u32[]{:S(2)}) copy-start(bf16[4096,256]{1,0:T(8,128)(2,1)} %param.17) | copy-start | bytes 6291460
  7.2 53.6 %all-gather.6.cloned.1.call-start = ((), (), s32[]{:S(2)}) async-start(), calls=%async_computation.5 | async-start | bytes 5242880 | tf_op jit(solution)/shard_map/all_gather | solution.py:54
  8.9 0.5 copy-start.10
  11.9 121.4 %all-gather.4.cloned.1.call-start = ((), (), s32[]{:S(2)}) async-start(), calls=%async_computation.4 | async-start | bytes 4718592 | tf_op jit(solution)/shard_map/all_gather | solution.py:104
  32.2 7.9 %copy-start.1 = (bf16[256,4096]{1,0:T(8,128)(2,1)S(1)}, bf16[256,4096]{1,0:T(8,128)(2,1)}, u32[]{:S(2)}) copy-start(bf16[256,4096]{1,0:T(8,128)(2,1)} %param.14) | copy-start | bytes 6291460
  32.2 8.4 %copy-start.6 = (f32[4096]{0:T(1024)S(1)}, f32[4096]{0:T(1024)}, u32[]{:S(2)}) copy-start(f32[4096]{0:T(1024)} %param.16) | copy-start | bytes 49156
  40.6 5.8 %copy-start.8 = (f32[256]{0:T(256)}, f32[256]{0:T(256)S(1)}, u32[]{:S(2)}) copy-start(f32[256]{0:T(256)S(1)} %add_rsqrt_fusion) | copy-start | bytes 3076
  59.8 160.5 %all-gather.8.cloned.1.call-start = ((), (), s32[]{:S(2)}) async-start(), calls=%async_computation.6 | async-start | bytes 5242880 | tf_op jit(solution)/shard_map/all_gather | solution.py:55
  60.5 284.9 %all-reduce.2.cloned.1.call-start = ((), (), s32[]{:S(2)}) async-start(), calls=%async_computation.9 | async-start | bytes 4194304 | tf_op jit(solution)/shard_map/psum | solution.py:145
  220.3 4.3 copy-start.4
  227.2 200.6 %reduce-scatter.5.cloned.1.call-start = ((), (), s32[]{:S(2)}) async-start(), calls=%async_computation.8 | async-start | bytes 4718592 | tf_op jit(solution)/shard_map/reduce_scatter | solution.py:134
  341.0 133.5 %reduce-scatter.3.cloned.1.call-start = ((), (), s32[]{:S(2)}) async-start(), calls=%async_computation.7 | async-start | bytes 5242880 | tf_op jit(solution)/shard_map/reduce_scatter | solution.py:146
  345.4 129.1 %copy-start.3 = (bf16[128,4096]{1,0:T(8,128)(2,1)S(1)}, bf16[128,4096]{1,0:T(8,128)(2,1)}, u32[]{:S(2)}) copy-start(bf16[128,4096]{1,0:T(8,128)(2,1)} %param.13) | copy-start | bytes 3145732
  345.4 129.1 %copy-start.5 = (f32[4096]{0:T(1024)S(1)}, f32[4096]{0:T(1024)}, u32[]{:S(2)}) copy-start(f32[4096]{0:T(1024)} %param.15) | copy-start | bytes 49156
  345.4 130.8 %copy-start.11 = (f32[128]{0:T(128)S(1)}, f32[128]{0:T(128)}, u32[]{:S(2)}) copy-start(f32[128]{0:T(128)} %copy-done.10) | copy-start | bytes 1540
  427.9 52.8 %copy-start.7 = (f32[4096]{0:T(1024)S(1)}, f32[4096]{0:T(1024)}, u32[]{:S(2)}) copy-start(f32[4096]{0:T(1024)} %param.16) | copy-start | bytes 49156
  427.9 51.5 %all-to-all-start.1 = ((bf16[4,256,256]{2,1,0:T(8,128)(2,1)}), bf16[4,256,256]{2,1,0:T(8,128)(2,1)}, u32[]{:S(2)}, u32[]{:S(2)}) async-start(bf16[4,256,256]{2,1,0:T(8,128)(2,1)} %bitcast.185), calls=%async_computation.3 | async-start | bytes 1048576 | tf_op jit(solution)/shard_map/all_to_all | solution.py:138
  480.6 7.2 %copy-start.2 = (bf16[256,4096]{1,0:T(8,128)(2,1)S(1)}, bf16[256,4096]{1,0:T(8,128)(2,1)}, u32[]{:S(2)}) copy-start(bf16[256,4096]{1,0:T(8,128)(2,1)} %param.14) | copy-start | bytes 6291460
  480.6 7.2 %copy-start.9 = (f32[256]{0:T(256)S(1)}, f32[256]{0:T(256)}, u32[]{:S(2)}) copy-start(f32[256]{0:T(256)} %copy-done.8) | copy-start | bytes 3076
Sparse Core Ops, SparseCore 0:
  12.0 37.1 all-gather.5
  59.9 73.3 all-gather.3
  134.9 32.9 all-gather.7
  227.3 100.8 all-reduce.1
  341.1 86.7 reduce-scatter.4
  430.2 44.2 reduce-scatter.2
where the time goes:
time: 501 us; the launch traced here: 498 us
  waiting for transfers between devices  189 us (38%)
  matrix products  142 us (28%)
  local copies, waits for them, and re-layouts  90.9 us (18%)
  other arithmetic  37.6 us (8%)
  between operations  14.4 us (3%)
  blocking collectives  13.2 us (3%)
  loops' own time  5.85 us (1%)
  starting transfers between devices  5.17 us (1%)
    reduce_scatter x1, waiting for transfers between devices, shards(): lax.psum_scatter(pair_store.astype(jnp.bfloat16), 'sp', scatter_dimension...  77.9 us
    all_gather x1, waiting for transfers between devices, shards(): lax.all_gather(own_pairs, 'sp', axis=0, tiled=True)  68.3 us
    reduce_scatter x1, waiting for transfers between devices, shards(): lax.psum_scatter(lax.dot_general(grad_query, w_query, contract_last, pref...  42.1 us
    dot_general x16, matrix products, score_block(): jnp.einsum('tkgd,skd->kgts', queries, key_block[:, :, 0], preferred_eleme...  39.8 us
    unnamed x27, local copies, waits for them, and re-layouts  33.4 us
    dot_general x8, matrix products, collect_advance(): jnp.einsum('kgts,skd->tkgd', mixed, key_block[:, :, 0], preferred_element...  20.8 us
    dot_general x8, matrix products, collect_advance(): jnp.einsum('kgts,tkgd->skd', mixed, queries, preferred_element_type=jnp.f...  18.6 us
    squeeze x16, local copies, waits for them, and re-layouts, shards(): lax.scan(absorb_advance, (start_max, start_sum, start_acc), blocks)  17.4 us
  transfers between devices with their start and end apart: 7, of which 3 were waited for; matrix products, arithmetic and copies ran while one was open for 50% of the time, Pallas kernels for 0%

commit v1 on v0

v1 whole, which is shorter than its diff:
```python
import functools
import math

import jax
import jax.numpy as jnp
from jax import lax
from jax.experimental import pallas as pl
from jax.experimental.pallas import tpu as pltpu
from jax.sharding import PartitionSpec as P

HD = 64
BLOCK = 512
LIMIT = 63000 * 1024


EPS = 1e-06


def normalize(matrix, scaling):
    widened = matrix.astype(jnp.float32)
    factor = lax.rsqrt(jnp.mean(widened * widened, axis=-1, keepdims=True) + EPS)
    return (widened * factor * scaling).astype(jnp.bfloat16)


def norm_back(matrix, scaling, upstream):
    widened = matrix.astype(jnp.float32)
    factor = lax.rsqrt(jnp.mean(widened * widened, axis=-1, keepdims=True) + EPS)
    weighted = upstream * scaling
    inner = jnp.mean(widened * weighted, axis=-1, keepdims=True)
    return factor * weighted - widened * factor * factor * factor * inner


def attend_kernel(key_count, group_size, block, q_ref, d_ref, kv_ref, o_ref, dq_ref, dkv_ref,
                  qpad, dpad, kvt, estore, mstore, ot, dqt):
    rows = q_ref.shape[0]
    width = kv_ref.shape[1]
    half = key_count * HD
    cols = group_size * rows
    blocks = kv_ref.shape[0] // block
    scale = float(HD) ** (-0.5)
    nt = (((1,), (1,)), ((), ()))
    nn = (((1,), (0,)), ((), ()))
    f32 = jnp.float32
    lane = lax.broadcasted_iota(jnp.int32, (rows, width), 1)
    qf = q_ref[...].astype(f32) * scale
    df = d_ref[...].astype(f32)
    if qf.shape[1] < width:
        qf = jnp.concatenate([qf] * (width // qf.shape[1]), axis=1)
        df = jnp.concatenate([df] * (width // df.shape[1]), axis=1)
    dt = d_ref[...].astype(f32).T
    for g in range(key_count):
        for j in range(group_size):
            h = g * group_size + j
            for source, store, base in ((qf, qpad, g * HD), (df, dpad, half + g * HD)):
                turn = (base - h * HD) % width
                moved = pltpu.roll(source, turn, 1) if turn else source
                keep = (lane >= base) & (lane < base + HD)
                store[g, j * rows:(j + 1) * rows, :] = jnp.where(keep, moved, 0.0).astype(jnp.bfloat16)

    def advance(i, state):
        here = pl.ds(pl.multiple_of(i * block, block), block)
        kvb = kv_ref[here, :]
        kvbt = kvb.astype(f32).T.astype(jnp.bfloat16)
        kvt[:, here] = kvbt
        out = []
        for g in range(key_count):
            m, l = state[2 * g], state[2 * g + 1]
            s = lax.dot_general(kvb, qpad[g], nt, preferred_element_type=f32)
            m_new = jnp.maximum(m, jnp.max(s, axis=0, keepdims=True))
            shrink = jnp.exp(m - m_new)
            e = jnp.exp(s - m_new)
            eb = e.astype(jnp.bfloat16)
            estore[g, here, :] = eb
            mstore[g, pl.ds(i, 1), :] = m_new
            l = l * shrink + jnp.sum(e, axis=0, keepdims=True)
            vt = kvbt[half + g * HD:half + (g + 1) * HD, :]
            ot[g] = ot[g] * shrink + lax.dot_general(vt, eb, nn, preferred_element_type=f32)
            out += [m_new, l]
        return tuple(out)

    ot[...] = jnp.zeros_like(ot)
    dqt[...] = jnp.zeros_like(dqt)
    start = []
    for g in range(key_count):
        start += [jnp.full((1, cols), -jnp.inf, f32), jnp.zeros((1, cols), f32)]
    state = lax.fori_loop(0, blocks, advance, tuple(start))

    deltas = []
    for g in range(key_count):
        inv = 1.0 / state[2 * g + 1]
        og = (ot[g] * inv).astype(jnp.bfloat16)
        ot[g] = og.astype(f32)
        parts = []
        for j in range(group_size):
            h = g * group_size + j
            parts.append(jnp.sum(dt[h * HD:(h + 1) * HD, :] * ot[g, :, j * rows:(j + 1) * rows], axis=0, keepdims=True))
        deltas.append(jnp.concatenate(parts, axis=1))
        mstore[g] = jnp.exp(mstore[g] - state[2 * g]) * inv
    pieces = [ot[g, :, j * rows:(j + 1) * rows] for g in range(key_count) for j in range(group_size)]
    o_ref[...] = jnp.concatenate(pieces, axis=0).T.astype(jnp.bfloat16)

    def collect(i, carry):
        here = pl.ds(pl.multiple_of(i * block, block), block)
        kvb = kv_ref[here, :]
        total = jnp.zeros((block, width), f32)
        for g in range(key_count):
            dp = lax.dot_general(kvb, dpad[g], nt, preferred_element_type=f32)
            p = estore[g, here, :].astype(f32) * mstore[g, pl.ds(i, 1), :]
            mixed = (p * (dp - deltas[g])).astype(jnp.bfloat16)
            total = total + lax.dot_general(mixed, qpad[g], nn, preferred_element_type=f32)
            total = total + lax.dot_general(p.astype(jnp.bfloat16), dpad[g], nn, preferred_element_type=f32)
            kt = kvt[g * HD:(g + 1) * HD, here]
            dqt[g] += lax.dot_general(kt, mixed, nn, preferred_element_type=f32)
        dkv_ref[here, :] = total.astype(jnp.bfloat16)
        return carry

    lax.fori_loop(0, blocks, collect, 0)
    pieces = [dqt[g, :, j * rows:(j + 1) * rows] for g in range(key_count) for j in range(group_size)]
    dq_ref[...] = (jnp.concatenate(pieces, axis=0) * scale).T.astype(jnp.bfloat16)


def attend(queries, grads, pairs, key_count, group_size):
    rows = queries.shape[0]
    source_rows, width = pairs.shape
    cols = group_size * rows
    block = math.gcd(source_rows, BLOCK)
    bf16, f32 = jnp.bfloat16, jnp.float32
    work = source_rows * cols * key_count * HD * 2
    whole = pl.BlockSpec(memory_space=pltpu.VMEM)
    return pl.pallas_call(
        functools.partial(attend_kernel, key_count, group_size, block),
        out_shape=(
            jax.ShapeDtypeStruct(queries.shape, bf16),
            jax.ShapeDtypeStruct(queries.shape, bf16),
            jax.ShapeDtypeStruct(pairs.shape, bf16),
        ),
        in_specs=[whole] * 3,
        out_specs=(whole,) * 3,
        scratch_shapes=[
            pltpu.VMEM((key_count, cols, width), bf16),
            pltpu.VMEM((key_count, cols, width), bf16),
            pltpu.VMEM((width, source_rows), bf16),
            pltpu.VMEM((key_count, source_rows, cols), bf16),
            pltpu.VMEM((key_count, source_rows // block, cols), f32),
            pltpu.VMEM((key_count, HD, cols), f32),
            pltpu.VMEM((key_count, HD, cols), f32),
        ],
        compiler_params=pltpu.CompilerParams(vmem_limit_bytes=LIMIT),
        cost_estimate=pl.CostEstimate(flops=6 * 4 * work, bytes_accessed=10 << 20, transcendentals=0),
        name="attend",
    )(queries, grads, pairs)


def shards(target, source, gain_target, gain_source, w_query, w_key, w_value, w_out, grad_output):
    contract_last = (((1,), (1,)), ((), ()))
    across = lax.axis_size("tp")
    heads_all = w_key.shape[1] // HD
    key_count = heads_all // across
    query_count = w_query.shape[1] // HD
    group_size = query_count // key_count
    normed_target = normalize(target, gain_target)
    normed_source = normalize(source, gain_source)
    gathered_target, gathered_grad = (
        lax.all_gather(normed_target, "tp", axis=0, tiled=True),
        lax.all_gather(grad_output, "tp", axis=0, tiled=True),
    )
    query = jnp.dot(gathered_target, w_query, preferred_element_type=jnp.float32).astype(
        jnp.bfloat16
    )
    head_grads = lax.dot_general(
        gathered_grad, w_out, contract_last, preferred_element_type=jnp.float32
    ).astype(jnp.bfloat16)
    keys_part = jnp.dot(normed_source, w_key, preferred_element_type=jnp.float32).astype(jnp.bfloat16)
    values_part = jnp.dot(normed_source, w_value, preferred_element_type=jnp.float32).astype(
        jnp.bfloat16
    )
    source_count = source.shape[0]
    pairs = jnp.concatenate(
        [
            keys_part.reshape(source_count, across, key_count * HD),
            values_part.reshape(source_count, across, key_count * HD),
        ],
        axis=2,
    ).reshape(source_count, across * 2 * key_count * HD)
    own_pairs = lax.all_to_all(pairs, "tp", split_axis=1, concat_axis=0, tiled=True)
    all_pairs = lax.all_gather(own_pairs, "sp", axis=0, tiled=True)
    attention, grad_query, pair_store = attend(query, head_grads, all_pairs, key_count, group_size)
    pair_grads = lax.psum_scatter(
        pair_store, "sp", scatter_dimension=0, tiled=True
    )
    pair_rows = lax.all_to_all(pair_grads, "tp", split_axis=0, concat_axis=1, tiled=True)
    split_rows = pair_rows.reshape(source_count, across, 2, key_count * HD)
    key_grads = split_rows[:, :, 0].reshape(source_count, heads_all * HD)
    value_grads = split_rows[:, :, 1].reshape(source_count, heads_all * HD)
    grad_sn = lax.dot_general(key_grads, w_key, contract_last, preferred_element_type=jnp.float32)
    grad_sn = grad_sn + lax.dot_general(
        value_grads, w_value, contract_last, preferred_element_type=jnp.float32
    )
    grad_source = norm_back(source, gain_source, grad_sn)
    proj_part = lax.dot_general(
        attention, gathered_grad, (((0,), (0,)), ((), ())), preferred_element_type=jnp.float32
    )
    grad_out_proj = lax.psum(proj_part.astype(jnp.bfloat16), "sp").astype(jnp.float32)
    grad_xn = lax.psum_scatter(
        lax.dot_general(
            grad_query, w_query, contract_last, preferred_element_type=jnp.float32
        ).astype(jnp.bfloat16),
        "tp",
        scatter_dimension=0,
        tiled=True,
    ).astype(jnp.float32)
    grad_target = norm_back(target, gain_target, grad_xn)
    return (grad_target, grad_source, grad_out_proj)


def solution(mesh):
    return jax.shard_map(
        shards,
        mesh=mesh,
        in_specs=(
            P(("sp", "tp"), None),
            P(("sp", "tp"), None),
            P(),
            P(),
            P(None, "tp"),
            P(),
            P(),
            P("tp", None),
            P(("sp", "tp"), None),
        ),
        out_specs=(P(("sp", "tp"), None), P(("sp", "tp"), None), P("tp", None)),
        check_vma=False,
    )
```

time: 501 us -> 509 us (1.016)
  waiting for transfers between devices: 189 us -> 343 us
  matrix products: 142 us -> 28 us
  local copies, waits for them, and re-layouts: 90.9 us -> 4.3 us
  Pallas kernels: 0 us -> 77.4 us
  other arithmetic: 37.6 us -> 18.5 us
  blocking collectives: 13.2 us -> 19.1 us
  loops' own time: 5.85 us -> 0 us
    dot_general x58 -> x4, matrix products: 127 us -> 10.9 us  [the longest x1 4.27 us: shards(): jnp.dot(normed_source, w_key, preferred_element_type=jnp.float32)]
    psum x1, waiting for transfers between devices: 0.02 us -> 96.8 us  [shards(): lax.psum(proj_part.astype(jnp.bfloat16), 'sp').astype(jnp.float32)]
    pallas_call x0 -> x1, Pallas kernels: none -> 77.4 us  [attend(): pl.pallas_call(functools.partial(attend_kernel, key_count, group_size, bl...]
    unnamed x27 -> x18, local copies, waits for them, and re-layouts: 33.4 us -> 1.1 us
    all_gather x1, waiting for transfers between devices: 0.02 us -> 31.9 us  [shards(): lax.all_gather(grad_output, 'tp', axis=0, tiled=True)]
    squeeze x16 -> x0, local copies, waits for them, and re-layouts: 17.4 us -> none  [shards(): lax.scan(absorb_advance, (start_max, start_sum, start_acc), blocks)]
    reshape x1, local copies, waits for them, and re-layouts: 15.1 us -> 0.09 us  [shards(): values_part.reshape(source_count, across, key_count * HD)]
    all_gather x1, waiting for transfers between devices: 0.02 us -> 14.8 us  [shards(): lax.all_gather(normed_target, 'tp', axis=0, tiled=True)]
  transfers between devices with their start and end apart: 7 -> 7, of which waited for: 3 -> 6; matrix products, arithmetic and copies ran while one was open for 50% -> 6% of each run, Pallas kernels for 0% -> 0%
where the time goes in v1:
time: 509 us
  waiting for transfers between devices  343 us (67%)
  Pallas kernels  77.4 us (15%)
  matrix products  28 us (6%)
  blocking collectives  19.1 us (4%)
  other arithmetic  18.5 us (4%)
  between operations  14.3 us (3%)
    psum x1, waiting for transfers between devices, shards(): lax.psum(proj_part.astype(jnp.bfloat16), 'sp').astype(jnp.float32)  96.8 us
    reduce_scatter x1, waiting for transfers between devices, shards(): lax.psum_scatter(pair_store, 'sp', scatter_dimension=0, tiled=True)  87.6 us
    pallas_call x1, Pallas kernels, attend(): pl.pallas_call(functools.partial(attend_kernel, key_count, group_size, bl...  77.4 us
    all_gather x1, waiting for transfers between devices, shards(): all_pairs = lax.all_gather(own_pairs, 'sp', axis=0, tiled=True)  70.1 us
    reduce_scatter x1, waiting for transfers between devices, shards(): lax.psum_scatter(lax.dot_general(grad_query, w_query, contract_last, pref...  40.5 us
    all_gather x1, waiting for transfers between devices, shards(): lax.all_gather(grad_output, 'tp', axis=0, tiled=True)  31.9 us
    all_to_all x1, blocking collectives, shards(): lax.all_to_all(pairs, 'tp', split_axis=1, concat_axis=0, tiled=True)  19.1 us
    all_gather x1, waiting for transfers between devices, shards(): lax.all_gather(normed_target, 'tp', axis=0, tiled=True)  14.8 us
  transfers between devices with their start and end apart: 7, of which 6 were waited for; matrix products, arithmetic and copies ran while one was open for 6% of the time, Pallas kernels for 0%

profile of v1, /device:TPU:0, one launch (start us, length us, event | category | flops | bytes accessed | tf_op | source)
XLA Modules:
  0.0 508.9 jit_solution(16669468998306372187)
XLA Ops:
  7.2 1.7 fusion.15
  8.9 2.5 fusion.11
  11.5 0.7 all-gather.6.cloned.1.call-update
  12.3 2.1 fusion.7
  14.4 4.3 fusion.17
  18.7 0.4 copy-done.4
  19.0 1.3 fusion.18
  20.5 19.1 %all_to_all.32 = bf16[256,4,256]{2,0,1:T(8,128)(2,1)} all-to-all(bf16[256,4,256]{2,0,1:T(8,128)(2,1)S(1)} %pad_maximum_fusion), channel_id=1, replica_groups=mesh['sp'=8,'tp'=4] {'tp'}, dimensions={1} | all-to-all | bytes 1048576 | tf_op jit(solution)/shard_map/all_to_all | solution.py:185
  39.6 14.8 %all-gather.4.cloned.1.call-done = bf16[512,4096]{1,0:T(8,128)(2,1)} async-done(((bf16[128,4096]{1,0:T(8,128)(2,1)}), bf16[512,4096]{1,0:T(8,128)(2,1)}) %all-gather.4.cloned.1.call-update) | async-done | bytes 4194320 | tf_op jit(solution)/shard_map/all_gather | solution.py:164
  54.4 4.1 convolution_convert_fusion.5.q_ref
  58.6 31.9 %all-gather.6.cloned.1.call-done = bf16[512,4096]{1,0:T(8,128)(2,1)} async-done(((bf16[128,4096]{1,0:T(8,128)(2,1)}), bf16[512,4096]{1,0:T(8,128)(2,1)}) %all-gather.6.cloned.1.call-update) | async-done | bytes 4194320 | tf_op jit(solution)/shard_map/all_gather | solution.py:165
  90.5 4.9 convolution_convert_fusion.4.d_ref
  95.3 70.1 %all-gather.8.cloned.1.call-done.kv_ref = bf16[8192,256]{1,0:T(8,128)(2,1)} async-done(((bf16[1024,256]{1,0:T(8,128)(2,1)}), bf16[8192,256]{1,0:T(8,128)(2,1)}) %all-gather.8.cloned.1.call-update) | async-done | bytes 4194320 | tf_op jit(solution)/shard_map/all_gather | solution.py:186
  165.4 77.4 %attend.1 = (bf16[512,256]{1,0:T(8,128)(2,1)}, bf16[512,256]{1,0:T(8,128)(2,1)}, bf16[8192,256]{1,0:T(8,128)(2,1)}) custom-call(bf16[512,256]{1,0:T(8,128)(2,1)} %convolution_convert_fusion.5.q_ref, bf16[512,256]{1,0:T(8,128)(2,1)} %convolution_convert_fusion.4.d_ref, bf16[8192,256]{1,0:T(8,128)(2,1)} %all-gather.8.cloned.1.call-done.kv_ref), custom_call_target="tpu_custom_call" | custom-call | flops 51539607552 | bytes 10485760 | tf_op jit(solution)/shard_map/attend/pallas_call | solution.py:130
  242.9 4.9 convolution_convert_fusion.1
  247.8 0.2 reduce-scatter.5.cloned.1.call-start
  248.0 0.4 reduce-scatter.5.cloned.1.call-update
  248.4 0.3 copy-done.6
  248.7 3.2 convolution_convert_fusion
  252.0 96.8 %all-reduce.2.cloned.1.call-done = bf16[256,4096]{1,0:T(8,128)(2,1)} async-done(((bf16[256,4096]{1,0:T(8,128)(2,1)}), bf16[256,4096]{1,0:T(8,128)(2,1)}) %all-reduce.2.cloned.1.call-update) | async-done | bytes 2097168 | tf_op jit(solution)/shard_map/psum | solution.py:203
  348.8 4.1 convert_element_type.49
  352.9 87.6 %reduce-scatter.5.cloned.1.call-done = bf16[1024,256]{1,0:T(8,128)(2,1)} async-done(((bf16[8192,256]{1,0:T(8,128)(2,1)}), bf16[1024,256]{1,0:T(8,128)(2,1)}) %reduce-scatter.5.cloned.1.call-update) | async-done | bytes 524304 | tf_op jit(solution)/shard_map/reduce_scatter | solution.py:188
  440.5 2.0 copy.18
  442.5 4.1 all-to-all-start.1
  446.7 40.5 %reduce-scatter.3.cloned.1.call-done = bf16[128,4096]{1,0:T(8,128)(2,1)} async-done(((bf16[512,4096]{1,0:T(8,128)(2,1)}), bf16[128,4096]{1,0:T(8,128)(2,1)}) %reduce-scatter.3.cloned.1.call-update) | async-done | bytes 1048592 | tf_op jit(solution)/shard_map/reduce_scatter | solution.py:204
  487.1 1.6 fusion.16
  488.8 3.2 fusion.14
  492.0 1.1 fusion.21
  493.1 3.6 fusion.22
  496.8 0.4 copy-done.5
  497.2 1.7 fusion.8
  498.8 3.2 fusion.6
  (31 shorter events, 0.5 us)
Async XLA Ops:
  7.2 47.2 %copy-start = (bf16[4096,256]{1,0:T(8,128)(2,1)S(1)}, bf16[4096,256]{1,0:T(8,128)(2,1)}, u32[]{:S(2)}) copy-start(bf16[4096,256]{1,0:T(8,128)(2,1)} %param.13) | copy-start | bytes 6291460
  7.2 7.2 %copy-start.8 = (f32[4096]{0:T(1024)S(1)}, f32[4096]{0:T(1024)}, u32[]{:S(2)}) copy-start(f32[4096]{0:T(1024)} %param.12) | copy-start | bytes 49156
  7.2 47.2 %all-gather.4.cloned.1.call-start = ((), (), s32[]{:S(2)}) async-start(), calls=%async_computation.4 | async-start | bytes 5242880 | tf_op jit(solution)/shard_map/all_gather | solution.py:164
  11.5 79.0 %all-gather.6.cloned.1.call-start = ((), (), s32[]{:S(2)}) async-start(), calls=%async_computation.5 | async-start | bytes 5242880 | tf_op jit(solution)/shard_map/all_gather | solution.py:165
  12.2 153.2 %all-gather.8.cloned.1.call-start = ((), (), s32[]{:S(2)}) async-start(), calls=%async_computation.6 | async-start | bytes 4718592 | tf_op jit(solution)/shard_map/all_gather | solution.py:186
  14.4 4.3 copy-start.1
  14.4 4.7 copy-start.4
  39.6 309.2 %all-reduce.2.cloned.1.call-start = ((), (), s32[]{:S(2)}) async-start(), calls=%async_computation.9 | async-start | bytes 4194304 | tf_op jit(solution)/shard_map/psum | solution.py:203
  247.7 0.9 copy-start.6
  247.8 192.7 %reduce-scatter.5.cloned.1.call-start = ((), (), s32[]{:S(2)}) async-start(), calls=%async_computation.8 | async-start | bytes 4718592 | tf_op jit(solution)/shard_map/reduce_scatter | solution.py:188
  248.3 238.8 %reduce-scatter.3.cloned.1.call-start = ((), (), s32[]{:S(2)}) async-start(), calls=%async_computation.7 | async-start | bytes 5242880 | tf_op jit(solution)/shard_map/reduce_scatter | solution.py:204
  251.9 235.2 %copy-start.3 = (bf16[128,4096]{1,0:T(8,128)(2,1)S(1)}, bf16[128,4096]{1,0:T(8,128)(2,1)}, u32[]{:S(2)}) copy-start(bf16[128,4096]{1,0:T(8,128)(2,1)} %param.9) | copy-start | bytes 3145732
  252.0 235.2 %copy-start.7 = (f32[4096]{0:T(1024)S(1)}, f32[4096]{0:T(1024)}, u32[]{:S(2)}) copy-start(f32[4096]{0:T(1024)} %param.11) | copy-start | bytes 49156
  442.5 49.5 %all-to-all-start.1 = ((bf16[4,256,256]{1,2,0:T(8,128)(2,1)}), bf16[4,256,256]{1,2,0:T(8,128)(2,1)}, u32[]{:S(2)}, u32[]{:S(2)}) async-start(bf16[4,256,256]{1,2,0:T(8,128)(2,1)} %copy.18), calls=%async_computation.3 | async-start | bytes 1048576 | tf_op jit(solution)/shard_map/all_to_all | solution.py:191
  493.1 3.7 copy-start.2
  493.1 4.1 copy-start.5
Sparse Core Ops, SparseCore 0:
  11.6 42.7 all-gather.3
  56.0 34.4 all-gather.5
  92.6 72.7 all-gather.7
  247.9 100.8 all-reduce.1
  352.8 87.6 reduce-scatter.4
  442.9 44.2 reduce-scatter.2
